TPU v7x, 512 devices: a whole 4x4x16 slice. The times are simulated.
512 devices in a mesh: sp: 64 (over z, y), tp: 8 (over x, core).
Axes of the slice: x: 4, y: 4, z: 16, core: 2. Of those that a mesh axis runs over, the one named last changes fastest.
Arguments:
- residual_signal: bfloat16 [16384, 2048], P('sp'), may hold values from -6 to 6
- reading_probe_preactivations: bfloat16 [16384, 1024], P('sp', 'tp'), may hold values from -6 to 6
- keep_switch_preactivations: bfloat16 [16384, 1024], P('sp', 'tp'), may hold values from -5.5 to 5.5
- written_entries: bfloat16 [16384, 1024], P('sp', 'tp'), may hold values from -6 to 6
- emission_switch_preactivations: bfloat16 [16384, 1024], P('sp', 'tp'), may hold values from -6 to 6
- additional_shrink_amount: float32 [16384, 1024], P('sp', 'tp'), may hold values from -0.7 to 0
- complement_of_floor: float32 [1024], P('tp'), may hold values from 6.1035156e-06 to 0.1
- per_group_rescaler: float32 [128], replicated, may hold values from 0.1 to 1.9
- emission_linear_map: bfloat16 [1024, 2048], P('tp'), may hold values from -0.1875 to 0.1875
- channel_layer_rescaler: float32 [2048], replicated, may hold values from 0.1 to 1.9
- expanding_linear_map: bfloat16 [2048, 8192], P('sp', 'tp'), may hold values from -0.125 to 0.125
- contracting_linear_map: bfloat16 [2048, 8192], P('sp', 'tp'), may hold values from -0.0625 to 0.0625
Outputs:
- layer_out: bfloat16 [16384, 2048], P('sp')
All inputs are finite; a program needn't handle non-finite values.
Results may differ from a plain program's by a relative error of at most 0.006.
Values may be sent and summed in bfloat16 or wider, within the bound.
A program may use at most 64 MiB of HBM per device.

v0:
```python
import jax
import jax.numpy as jnp
from jax import lax
from jax.sharding import Mesh
from jax.sharding import PartitionSpec as P

HEAD = 128
BLOCK = 64
SP = ("sp_0", "sp_1")
norm_eps = 1e-06
HIGH_ACCURACY = lax.Precision.HIGHEST


def filled_with(shard, identity):
    return jax.tree.map(
        lambda a, e: jnp.broadcast_to(jnp.asarray(e, a.dtype), a.shape), shard, identity
    )


def gathered_once(shard, axis):
    leaves = jax.tree.leaves(shard)
    turns = sorted(range(len(leaves)), key=lambda k: -leaves[k].size)
    width = (1, *leaves[turns[0]].shape)[-1]
    lines = [
        jnp.pad(leaves[k].reshape(-1), (0, -leaves[k].size % width)).reshape(-1, width)
        for k in turns
    ]
    both, at, found = (lax.all_gather(jnp.concatenate(lines), axis), 0, {})
    for k, line in zip(turns, lines):
        piece = both[:, at : at + len(line)].reshape(len(both), -1)
        found[k] = piece[:, : leaves[k].size].reshape(-1, *leaves[k].shape)
        at += len(line)
    numbers = iter(range(len(leaves)))
    return jax.tree.map(lambda _: found[next(numbers)], shard)


def entering(shard, axes, combine, identity):
    before = start = filled_with(shard, identity)
    total = shard
    for axis in reversed(axes):
        peers, index = (lax.axis_size(axis), lax.axis_index(axis))
        pieces = gathered_once(total, axis)
        inside, total = (start, start)
        for k in range(peers):
            passed = k < index
            total = combine(total, jax.tree.map(lambda part: part[k], pieces))
            inside = jax.tree.map(lambda new, old: jnp.where(passed, new, old), total, inside)
        before = combine(inside, before)
    return before


def laid_out(blocks, dim):
    lengths = list(blocks.shape[1:])
    lengths[dim] *= blocks.shape[0]
    return jnp.moveaxis(blocks, 0, dim).reshape(lengths)


def copy_for_each(shard, axis):
    peers = lax.axis_size(axis)
    return lax.all_to_all(
        jnp.broadcast_to(shard[None], (peers, *shard.shape)), axis, 0, 0, tiled=True
    )


def gathered_copies(shard, axis, dim):
    return laid_out(copy_for_each(shard, axis), dim)


def in_one_piece(arrays, axis, dim, along):
    widths = [a.shape[along] for a in arrays]
    both = jnp.concatenate(arrays, axis=along)
    whole = lax.all_gather(both, axis, axis=dim, tiled=True)
    return tuple(jnp.split(whole, [sum(widths[:k]) for k in range(1, len(widths))], axis=along))


def cut_along(shard, dim, peers):
    lengths = shard.shape
    blocks = shard.reshape(*lengths[:dim], peers, lengths[dim] // peers, *lengths[dim + 1 :])
    return jnp.moveaxis(blocks, dim, 0)


def sum_at_owner(shard, axis, dim):
    blocks = cut_along(shard, dim, lax.axis_size(axis))
    arrived = lax.all_to_all(blocks, axis, split_axis=0, concat_axis=0, tiled=True)
    return arrived.astype(jnp.float32).sum(axis=0)


def block_step(state_matrix, inputs):
    query_block_rows, key_blk, logs_blk, value_block_rows = inputs
    cumulative_decay = jnp.cumsum(logs_blk, axis=1)
    carried_state = jnp.einsum(
        "rlb,rbz->rlz",
        query_block_rows * jnp.exp(cumulative_decay),
        state_matrix,
        precision=HIGH_ACCURACY,
    )
    spread = cumulative_decay[:, :, None, :] - cumulative_decay[:, None, :, :]
    places = jnp.arange(BLOCK)
    lower = places[:, None] >= places[None, :]
    decay = jnp.exp(jnp.where(lower[None, :, :, None], spread, -jnp.inf))
    scores = jnp.einsum(
        "htk,hsk,htsk->hts", query_block_rows, key_blk, decay, precision=HIGH_ACCURACY
    )
    result = carried_state + jnp.einsum(
        "hts,hsv->htv", scores, value_block_rows, precision=HIGH_ACCURACY
    )
    final_state = cumulative_decay[:, -1:, :]
    decayed_key_rows = key_blk * jnp.exp(final_state - cumulative_decay)
    state_matrix = jnp.exp(final_state[:, 0, :])[..., None] * state_matrix + jnp.einsum(
        "aux,auf->axf", decayed_key_rows, value_block_rows, precision=HIGH_ACCURACY
    )
    return (state_matrix, result)


def combine_carry(earlier, later):
    return (earlier[0] * later[0], later[0][..., None] * earlier[1] + later[1])


def body(
    residual_signal,
    reading_probe_preactivations,
    keep_switch_preactivations,
    written_entries,
    emission_switch_preactivations,
    additional_shrink_amount,
    complement_of_floor,
    per_group_rescaler,
    emission_linear_map,
    channel_layer_rescaler,
    expanding_linear_map,
    contracting_linear_map,
):
    positions = reading_probe_preactivations.shape[0]
    channels = reading_probe_preactivations.shape[1]
    local_heads = channels // HEAD
    count = positions // BLOCK
    query_act = jax.nn.silu(reading_probe_preactivations.astype(jnp.float32))
    logarithmic_keep_fraction = (
        jnp.logaddexp(
            jnp.log1p(-complement_of_floor),
            jnp.log(complement_of_floor)
            + jax.nn.log_sigmoid(keep_switch_preactivations.astype(jnp.float32)),
        )
        + additional_shrink_amount
    )
    key_part = -jnp.expm1(logarithmic_keep_fraction)
    value_part = written_entries.astype(jnp.float32)

    def to_blocks(values):
        return values.reshape(count, BLOCK, local_heads, HEAD).transpose(0, 2, 1, 3)

    start = jnp.zeros((local_heads, HEAD, HEAD), jnp.float32)
    state_end, outputs = lax.scan(
        block_step,
        start,
        (
            to_blocks(query_act),
            to_blocks(key_part),
            to_blocks(logarithmic_keep_fraction),
            to_blocks(value_part),
        ),
    )
    within_block_output = outputs.transpose(0, 2, 1, 3).reshape(positions, local_heads, HEAD)
    running = jnp.cumsum(logarithmic_keep_fraction, axis=0)
    decay_total = jnp.exp(running[-1]).reshape(local_heads, HEAD)
    identity = (
        jnp.ones((local_heads, HEAD), jnp.float32),
        jnp.zeros((local_heads, HEAD, HEAD), jnp.float32),
    )
    prior_state = entering((decay_total, state_end), SP, combine_carry, identity)
    weighted_scores = (query_act * jnp.exp(running)).reshape(positions, local_heads, HEAD)
    recurrent_output = within_block_output + jnp.einsum(
        "pnm,nmx->pnx", weighted_scores, prior_state[1], precision=HIGH_ACCURACY
    )
    scaled = (
        recurrent_output
        * lax.rsqrt(
            jnp.mean(recurrent_output * recurrent_output, axis=-1, keepdims=True) + norm_eps
        )
        * per_group_rescaler
    )
    gated = scaled * jax.nn.silu(emission_switch_preactivations.astype(jnp.float32)).reshape(
        positions, local_heads, HEAD
    )
    mixed_heads = gated.reshape(positions, channels).astype(jnp.bfloat16)
    all_heads = gathered_copies(mixed_heads, "tp", 1)
    full_out = lax.all_gather(emission_linear_map, "tp", axis=0, tiled=True)
    projected = jnp.dot(all_heads, full_out, preferred_element_type=jnp.float32)
    after_mix = residual_signal.astype(jnp.float32) + projected
    normed = (
        after_mix
        * lax.rsqrt(jnp.mean(after_mix * after_mix, axis=-1, keepdims=True) + norm_eps)
        * channel_layer_rescaler
    ).astype(jnp.bfloat16)
    up_whole, down_whole = in_one_piece((expanding_linear_map, contracting_linear_map), SP, 0, 1)
    upward = jnp.dot(normed, up_whole, preferred_element_type=jnp.float32)
    hidden = jnp.square(jax.nn.relu(upward)).astype(jnp.bfloat16)
    share = positions // lax.axis_size("tp")
    downward = sum_at_owner(
        lax.dot_general(
            hidden, down_whole, (((1,), (1,)), ((), ())), preferred_element_type=jnp.float32
        ).astype(jnp.bfloat16),
        "tp",
        0,
    )
    own_start = lax.axis_index("tp") * share
    own_mix = lax.dynamic_slice_in_dim(after_mix, own_start, share, 0)
    finished = (own_mix + downward).astype(jnp.bfloat16)
    return gathered_copies(finished, "tp", 0)


def solution(mesh):
    finer = Mesh(mesh.devices.reshape(16, 4, mesh.shape["tp"]), ("sp_0", "sp_1", "tp"))
    return jax.shard_map(
        body,
        mesh=finer,
        in_specs=(
            P(SP, None),
            P(SP, "tp"),
            P(SP, "tp"),
            P(SP, "tp"),
            P(SP, "tp"),
            P(SP, "tp"),
            P("tp"),
            P(),
            P("tp", None),
            P(),
            P(SP, "tp"),
            P(SP, "tp"),
        ),
        out_specs=P(SP, None),
        check_vma=False,
    )
```

profile of v0, /device:TPU:1, one launch (start us, length us, event | category | flops | bytes accessed | tf_op | source)
XLA Modules:
  0.0 363.2 jit_solution(13176499211492240413)
XLA Ops:
  6.5 0.7 negate_log-plus-one_fusion
  7.2 1.1 exponential-minus-one_negate_fusion
  8.4 0.1 fusion.63
  8.6 0.1 copy.45
  8.9 1.0 copy.41
  10.1 13.1 %while.13 = (s32[]{:T(128)}, f32[1,128,128]{2,1,0:T(8,128)S(1)}, f32[4,1,64,128]{3,2,1,0:T(8,128)S(1)}, f32[4,1,64,128]{3,2,1,0:T(8,128)S(1)}, f32[4,1,64,128]{3...) while((s32[]{:T(128)}, f32[1,128,128]{2,1,0:T(8,128)S(1)}, ...), condition=%wide.region_2.3_spmd.clone, body=%wide.region_0.2_spmd.clone.sunk | while | flops 34693120 | bytes 5108864 | solution.py:153
  10.1 0.1 reduce_window_sum.34
  10.2 0.6 select_exponential_fusion.2
  10.8 1.7 fusion.174
  12.6 0.2 fusion.173
  12.7 0.2 fusion.175
  13.0 0.3 fusion.172
  13.4 0.1 reduce_window_sum.34
  13.5 0.6 select_exponential_fusion.2
  14.1 1.7 fusion.174
  15.8 0.2 fusion.173
  16.0 0.2 fusion.175
  16.3 0.3 fusion.172
  16.7 0.6 select_exponential_fusion.2
  17.4 1.7 fusion.174
  19.1 0.2 fusion.173
  19.3 0.2 fusion.175
  19.5 0.3 fusion.172
  20.0 0.6 select_exponential_fusion.2
  20.6 1.7 fusion.174
  22.4 0.2 fusion.173
  22.5 0.2 fusion.175
  22.8 0.3 fusion.172
  23.2 10.7 %all-gather.2 = f32[4,129,128]{2,1,0:T(8,128)S(1)} all-gather(f32[1,129,128]{2,1,0:T(8,128)S(1)} %maximum_bitcast_fusion), channel_id=2, replica_groups=mesh['sp_0'=16,'sp_1'=4,'tp'=8] {'sp_1'}, dimensions={0}, use_global_device_ids=true | all-gather | bytes 330240 | tf_op jit(solution)/shard_map/all_gather | solution.py:28
  33.9 0.1 fusion.153
  34.1 0.6 maximum_bitcast_fusion.1
  34.8 0.7 all-gather.8.cloned.1.call-update
  35.6 0.7 pad_maximum_fusion
  36.4 0.1 copy.48
  36.5 65.5 %all-gather.12.cloned.1.call-done = f32[16,129,128]{2,1,0:T(8,128)} async-done(((f32[1,129,128]{2,1,0:T(8,128)}), f32[16,129,128]{2,1,0:T(8,128)}) %all-gather.12.cloned.1.call-update) | async-done | bytes 1056784 | tf_op jit(solution)/shard_map/all_gather | solution.py:28
  102.1 0.8 slice_bitcast_fusion.16
  102.8 2.1 multiply_reduce_fusion.1
  105.1 24.3 %all_to_all.15 = bf16[8,256,128]{1,2,0:T(8,128)(2,1)S(1)} all-to-all(bf16[8,256,128]{1,2,0:T(8,128)(2,1)S(1)} %broadcast_in_dim.32), channel_id=1, replica_groups=mesh['sp_0'=16,'sp_1'=4,'tp'=8] {'tp'}, dimensions={0} | all-to-all | bytes 1048576 | tf_op jit(solution)/shard_map/all_to_all | solution.py:60
  129.4 22.2 %all-gather.8.cloned.1.call-done = bf16[1024,2048]{1,0:T(8,128)(2,1)} async-done(((bf16[128,2048]{1,0:T(8,128)(2,1)}), bf16[1024,2048]{1,0:T(8,128)(2,1)}) %all-gather.8.cloned.1.call-update) | async-done | bytes 4194320 | tf_op jit(solution)/shard_map/all_gather | solution.py:187
  151.7 3.9 %multiply_reduce_fusion = (f32[256]{0:T(256)S(1)}, f32[256,2048]{1,0:T(8,128)S(1)}) fusion(bf16[256,1024]{0,1:T(8,128)(2,1)S(1)} %bitcast.218, bf16[1024,2048]{1,0:T(8,128)(2,1)} %all-gather.8.cloned.1.call-done, bf16[256,2048]{1,0:T(8,128)(2,1)} %param.14), kind=kOutput, calls=%fused_computation.45 | convolution fusion | flops 1075838720 | bytes 7865344 | tf_op jit(solution)/shard_map/dot_general | solution.py:188
  155.5 147.1 %all-gather.10.cloned.1.call-done = bf16[2048,2048]{1,0:T(8,128)(2,1)} async-done(((bf16[32,2048]{1,0:T(8,128)(2,1)}), bf16[2048,2048]{1,0:T(8,128)(2,1)}) %all-gather.10.cloned.1.call-update) | async-done | bytes 8388624 | tf_op jit(solution)/shard_map/all_gather | solution.py:72
  302.7 6.8 %fusion.32 = bf16[256,2048]{1,0:T(8,128)(2,1)} fusion(bf16[2048,2048]{1,0:T(8,128)(2,1)} %all-gather.10.cloned.1.call-done, f32[256,2048]{1,0:T(8,128)S(1)} %get-tuple-element.142, f32[2048]{0:T(1024)S(1)} %copy-done.5, f32[256]{0:T(256)S(1)} %add_rsqrt_fusion), kind=kOutput, calls=%fused_computation.42 | convolution fusion | flops 2150367232 | bytes 11543552 | tf_op jit(solution)/shard_map/dot_general | solution.py:200
  309.5 12.7 %all-to-all-start.1 = ((bf16[8,32,2048]{2,1,0:T(8,128)(2,1)}), bf16[8,32,2048]{2,1,0:T(8,128)(2,1)S(1)}, u32[]{:S(2)}, u32[]{:S(2)}) async-start(bf16[8,32,2048]{2,1,0:T(8,128)(2,1)} %bitcast.223), calls=%async_computation.1 | async-start | bytes 2097152 | tf_op jit(solution)/shard_map/all_to_all | solution.py:84
  322.2 15.0 %all-to-all-done.1 = bf16[8,32,2048]{2,1,0:T(8,128)(2,1)S(1)} async-done(((bf16[8,32,2048]{2,1,0:T(8,128)(2,1)}), bf16[8,32,2048]{2,1,0:T(8,128)(2,1)S(1)}, u32[]{:S(2)}, u32[]{:S(2)}) %all-to-all-start.1) | async-done | bytes 1048608 | tf_op jit(solution)/shard_map/all_to_all | solution.py:84
  337.1 0.1 convert_reduce_fusion
  337.3 0.1 broadcast_in_dim.33
  337.4 18.3 %all_to_all.16 = bf16[8,32,2048]{2,1,0:T(8,128)(2,1)S(1)} all-to-all(bf16[8,32,2048]{2,1,0:T(8,128)(2,1)S(1)} %broadcast_in_dim.33), channel_id=1, replica_groups=mesh['sp_0'=16,'sp_1'=4,'tp'=8] {'tp'}, dimensions={0} | all-to-all | bytes 2097152 | tf_op jit(solution)/shard_map/all_to_all | solution.py:60
  355.7 1.0 copy.80
  (62 shorter events, 1.2 us)
Async XLA Ops:
  6.5 3.5 copy-start
  6.5 95.5 %all-gather.12.cloned.1.call-start = ((), (), s32[]{:S(2)}) async-start(), calls=%async_computation.5 | async-start | bytes 1183744 | tf_op jit(solution)/shard_map/all_gather | solution.py:28
  10.0 25.5 %copy-start.2 = (bf16[32,1024]{1,0:T(8,128)(2,1)S(1)}, bf16[32,1024]{1,0:T(8,128)(2,1)}, u32[]{:S(2)}) copy-start(bf16[32,1024]{1,0:T(8,128)(2,1)} %param.25) | copy-start | bytes 196612
  10.1 25.5 %copy-start.3 = (bf16[32,1024]{1,0:T(8,128)(2,1)S(1)}, bf16[32,1024]{1,0:T(8,128)(2,1)}, u32[]{:S(2)}) copy-start(bf16[32,1024]{1,0:T(8,128)(2,1)} %param.24) | copy-start | bytes 196612
  23.1 13.3 %copy-start.1 = (bf16[256,128]{1,0:T(8,128)(2,1)S(1)}, bf16[256,128]{1,0:T(8,128)(2,1)}, u32[]{:S(2)}) copy-start(bf16[256,128]{1,0:T(8,128)(2,1)} %param.18) | copy-start | bytes 196612
  34.7 70.2 %copy-start.4 = (f32[128]{0:T(128)S(1)}, f32[128]{0:T(128)}, u32[]{:S(2)}) copy-start(f32[128]{0:T(128)} %param.21) | copy-start | bytes 1540
  34.7 116.9 %all-gather.8.cloned.1.call-start = ((), (), s32[]{:S(2)}) async-start(), calls=%async_computation.3 | async-start | bytes 4718592 | tf_op jit(solution)/shard_map/all_gather | solution.py:187
  35.5 267.2 %all-gather.10.cloned.1.call-start = ((), (), s32[]{:S(2)}) async-start(), calls=%async_computation.4 | async-start | bytes 8519680 | tf_op jit(solution)/shard_map/all_gather | solution.py:72
  151.7 151.0 %copy-start.5 = (f32[2048]{0:T(1024)S(1)}, f32[2048]{0:T(1024)}, u32[]{:S(2)}) copy-start(f32[2048]{0:T(1024)} %param.23) | copy-start | bytes 24580
  309.5 27.6 %all-to-all-start.1 = ((bf16[8,32,2048]{2,1,0:T(8,128)(2,1)}), bf16[8,32,2048]{2,1,0:T(8,128)(2,1)S(1)}, u32[]{:S(2)}, u32[]{:S(2)}) async-start(bf16[8,32,2048]{2,1,0:T(8,128)(2,1)} %bitcast.223), calls=%async_computation.1 | async-start | bytes 2097152 | tf_op jit(solution)/shard_map/all_to_all | solution.py:84
Sparse Core Ops, SparseCore 0:
  34.8 67.1 all-gather.11
  104.2 47.3 all-gather.7
  154.6 148.0 all-gather.9
where the time goes:
time: 364 us; the launch traced here: 363 us
  waiting for transfers between devices  251 us (69%)
  blocking collectives  53.4 us (15%)
  matrix products  15.7 us (4%)
  other arithmetic  14.3 us (4%)
  between operations  13.4 us (4%)
  starting transfers between devices  12.8 us (4%)
    all_gather x1, waiting for transfers between devices, in_one_piece(): whole = lax.all_gather(both, axis, axis=dim, tiled=True)  147 us
    all_gather x1, waiting for transfers between devices, gathered_once(): both, at, found = (lax.all_gather(jnp.concatenate(lines), axis), 0, {})  65.5 us
    all_to_all x2, blocking collectives, copy_for_each(): lax.all_to_all(jnp.broadcast_to(shard[None], (peers, *shard.shape)), axis...  42.6 us
    all_gather x1, waiting for transfers between devices, body(): full_out = lax.all_gather(emission_linear_map, 'tp', axis=0, tiled=True)  22.2 us
    all_to_all x1, waiting for transfers between devices, sum_at_owner(): lax.all_to_all(blocks, axis, split_axis=0, concat_axis=0, tiled=True)  15 us
    all_to_all x1, starting transfers between devices, sum_at_owner(): lax.all_to_all(blocks, axis, split_axis=0, concat_axis=0, tiled=True)  12.7 us
    all_gather x1, blocking collectives, gathered_once(): both, at, found = (lax.all_gather(jnp.concatenate(lines), axis), 0, {})  10.7 us
  transfers between devices with their start and end apart: 4, of which 4 were waited for; matrix products, arithmetic and copies ran while one was open for 2% of the time, Pallas kernels for 0%

commit v1 on v0

--- a/solution.py
+++ b/solution.py
@@ -9,6 +9,16 @@
 SP = ("sp_0", "sp_1")
 norm_eps = 1e-06
 HIGH_ACCURACY = lax.Precision.HIGHEST
+
+
+def gather_by_hops(block, axis, dim):
+    count = lax.axis_size(axis)
+    moving, pieces = (block, [block])
+    for _ in range(count - 1):
+        moving = lax.ppermute(moving, axis, [(i, (i + 1) % count) for i in range(count)])
+        pieces.insert(0, moving)
+    line = jnp.concatenate(pieces, axis=dim)
+    return jnp.roll(line, (lax.axis_index(axis) + 1) * block.shape[dim], axis=dim)
 
 
 def filled_with(shard, identity):
@@ -184,7 +194,7 @@
     )
     mixed_heads = gated.reshape(positions, channels).astype(jnp.bfloat16)
     all_heads = gathered_copies(mixed_heads, "tp", 1)
-    full_out = lax.all_gather(emission_linear_map, "tp", axis=0, tiled=True)
+    full_out = gather_by_hops(emission_linear_map, "tp", 0)
     projected = jnp.dot(all_heads, full_out, preferred_element_type=jnp.float32)
     after_mix = residual_signal.astype(jnp.float32) + projected
     normed = (

time: 364 us -> 327 us (0.90)
  waiting for transfers between devices: 251 us -> 184 us
  starting transfers between devices: 12.8 us -> 38.9 us
  blocking collectives: 53.4 us -> 29.1 us
  local copies, waits for them, and re-layouts: 2.83 us -> 24.5 us
    all_gather x1, waiting for transfers between devices: 65.5 us -> 14.9 us  [gathered_once(): both, at, found = (lax.all_gather(jnp.concatenate(lines), axis), 0, {})]
    ppermute x0 -> x7, waiting for transfers between devices: none -> 38.6 us  [gather_by_hops(): lax.ppermute(moving, axis, [(i, (i + 1) % count) for i in range(count)])]
    all_gather x1, waiting for transfers between devices: 147 us -> 116 us  [in_one_piece(): whole = lax.all_gather(both, axis, axis=dim, tiled=True)]
    all_to_all x2 -> x1, blocking collectives: 42.6 us -> 18.3 us  [copy_for_each(): lax.all_to_all(jnp.broadcast_to(shard[None], (peers, *shard.shape)), axis...]
    all_gather x1 -> x0, waiting for transfers between devices: 22.2 us -> none  [body(): full_out = lax.all_gather(emission_linear_map, 'tp', axis=0, tiled=True)]
    ppermute x0 -> x7, starting transfers between devices: none -> 22.1 us  [gather_by_hops(): lax.ppermute(moving, axis, [(i, (i + 1) % count) for i in range(count)])]
    unnamed x17 -> x40, local copies, waits for them, and re-layouts: 2.1 us -> 20.6 us
    all_to_all x0 -> x1, starting transfers between devices: none -> 4.11 us  [copy_for_each(): lax.all_to_all(jnp.broadcast_to(shard[None], (peers, *shard.shape)), axis...]
  transfers between devices with their start and end apart: 4 -> 11, of which waited for: 4 -> 8; matrix products, arithmetic and copies ran while one was open for 2% -> 9% of each run, Pallas kernels for 0% -> 0%
where the time goes in v1:
time: 327 us
  waiting for transfers between devices  184 us (56%)
  starting transfers between devices  38.9 us (12%)
  blocking collectives  29.1 us (9%)
  local copies, waits for them, and re-layouts  24.5 us (7%)
  matrix products  18.4 us (6%)
  other arithmetic  17.3 us (5%)
  between operations  13.7 us (4%)
    all_gather x1, waiting for transfers between devices, in_one_piece(): whole = lax.all_gather(both, axis, axis=dim, tiled=True)  116 us
    ppermute x7, waiting for transfers between devices, gather_by_hops(): lax.ppermute(moving, axis, [(i, (i + 1) % count) for i in range(count)])  38.6 us
    ppermute x7, starting transfers between devices, gather_by_hops(): lax.ppermute(moving, axis, [(i, (i + 1) % count) for i in range(count)])  22.1 us
    unnamed x40, local copies, waits for them, and re-layouts  20.6 us
    all_to_all x1, blocking collectives, copy_for_each(): lax.all_to_all(jnp.broadcast_to(shard[None], (peers, *shard.shape)), axis...  18.3 us
    all_to_all x1, waiting for transfers between devices, sum_at_owner(): lax.all_to_all(blocks, axis, split_axis=0, concat_axis=0, tiled=True)  15 us
    all_gather x1, waiting for transfers between devices, gathered_once(): both, at, found = (lax.all_gather(jnp.concatenate(lines), axis), 0, {})  14.9 us
    all_to_all x1, starting transfers between devices, sum_at_owner(): lax.all_to_all(blocks, axis, split_axis=0, concat_axis=0, tiled=True)  12.7 us
  transfers between devices with their start and end apart: 11, of which 8 were waited for; matrix products, arithmetic and copies ran while one was open for 9% of the time, Pallas kernels for 0%

profile of v1, /device:TPU:1, one launch (start us, length us, event | category | flops | bytes accessed | tf_op | source)
XLA Modules:
  0.0 326.5 jit_solution(3775686925104905795)
XLA Ops:
  7.2 1.1 exponential-minus-one_negate_fusion
  8.8 1.0 copy.41
  10.0 0.9 convert.1
  10.9 15.5 %while.13 = (s32[]{:T(128)}, f32[1,128,128]{2,1,0:T(8,128)S(1)}, f32[4,1,64,128]{3,2,1,0:T(8,128)}, f32[4,1,64,128]{3,2,1,0:T(8,128)S(1)}, f32[4,1,64,128]{3,2,1...) while((s32[]{:T(128)}, f32[1,128,128]{2,1,0:T(8,128)S(1)}, ...), condition=%wide.region_2.3_spmd.clone, body=%wide.region_0.2_spmd.clone.sunk | while | flops 34693120 | bytes 5108864 | solution.py:163
  11.7 1.7 fusion.179
  13.6 0.9 fusion.180
  15.5 1.7 fusion.179
  17.4 0.9 fusion.180
  19.4 1.7 fusion.179
  21.3 0.9 fusion.180
  23.3 1.7 fusion.179
  25.2 0.9 fusion.180
  26.4 10.7 %all-gather.2 = f32[4,129,128]{2,1,0:T(8,128)S(1)} all-gather(f32[1,129,128]{2,1,0:T(8,128)S(1)} %maximum_bitcast_fusion), channel_id=2, replica_groups=mesh['sp_0'=16,'sp_1'=4,'tp'=8] {'sp_1'}, dimensions={0}, use_global_device_ids=true | all-gather | bytes 330240 | tf_op jit(solution)/shard_map/all_gather | solution.py:38
  39.2 4.7 %collective-permute-start = (bf16[128,2048]{1,0:T(8,128)(2,1)S(1)}, bf16[128,2048]{1,0:T(8,128)(2,1)S(1)}, u32[]{:S(2)}, u32[]{:S(2)}) collective-permute-start(bf16[128,2048]{1,0:T(8,128)(2,1)S(1)} %copy-done), channel_id=1, source_target_pairs={{0,1},{1,2},{2,3},{3,4},{4,5},{5,6},{6,7},{7,0},{8,9},{9,10},{10,1... | collective-permute-start | bytes 1572872 | tf_op jit(solution)/shard_map/ppermute | solution.py:18
  43.9 6.1 %collective-permute-done = bf16[128,2048]{1,0:T(8,128)(2,1)S(1)} collective-permute-done((bf16[128,2048]{1,0:T(8,128)(2,1)S(1)}, bf16[128,2048]{1,0:T(8,128)(2,1)S(1)}, u32[]{:S(2)}, u32[]{:S(2)}) %collective-permute-start) | collective-permute-done | bytes 524320 | tf_op jit(solution)/shard_map/ppermute | solution.py:18
  50.0 2.5 collective-permute-start.1
  52.5 6.3 %collective-permute-done.1 = bf16[128,2048]{1,0:T(8,128)(2,1)S(1)} collective-permute-done((bf16[128,2048]{1,0:T(8,128)(2,1)S(1)}, bf16[128,2048]{1,0:T(8,128)(2,1)S(1)}, u32[]{:S(2)}, u32[]{:S(2)}) %collective-permute-start.1) | collective-permute-done | bytes 524320 | tf_op jit(solution)/shard_map/ppermute | solution.py:18
  58.8 2.3 collective-permute-start.2
  61.1 7.6 %collective-permute-done.2 = bf16[128,2048]{1,0:T(8,128)(2,1)S(1)} collective-permute-done((bf16[128,2048]{1,0:T(8,128)(2,1)S(1)}, bf16[128,2048]{1,0:T(8,128)(2,1)S(1)}, u32[]{:S(2)}, u32[]{:S(2)}) %collective-permute-start.2) | collective-permute-done | bytes 524320 | tf_op jit(solution)/shard_map/ppermute | solution.py:18
  68.6 1.1 collective-permute-start.3
  69.7 8.8 %collective-permute-done.3 = bf16[128,2048]{1,0:T(8,128)(2,1)S(1)} collective-permute-done((bf16[128,2048]{1,0:T(8,128)(2,1)S(1)}, bf16[128,2048]{1,0:T(8,128)(2,1)S(1)}, u32[]{:S(2)}, u32[]{:S(2)}) %collective-permute-start.3) | collective-permute-done | bytes 524320 | tf_op jit(solution)/shard_map/ppermute | solution.py:18
  78.5 9.8 %collective-permute-done.4 = bf16[128,2048]{1,0:T(8,128)(2,1)S(1)} collective-permute-done((bf16[128,2048]{1,0:T(8,128)(2,1)S(1)}, bf16[128,2048]{1,0:T(8,128)(2,1)S(1)}, u32[]{:S(2)}, u32[]{:S(2)}) %collective-permute-start.4) | collective-permute-done | bytes 524320 | tf_op jit(solution)/shard_map/ppermute | solution.py:18
  88.3 1.6 copy.47
  89.9 1.6 copy.48
  91.5 14.9 %all-gather.9.cloned.1.call-done = f32[16,129,128]{2,1,0:T(8,128)} async-done(((f32[1,129,128]{2,1,0:T(8,128)}), f32[16,129,128]{2,1,0:T(8,128)}) %all-gather.9.cloned.1.call-update) | async-done | bytes 1056784 | tf_op jit(solution)/shard_map/all_gather | solution.py:38
  107.2 11.6 %collective-permute-start.6 = (bf16[128,2048]{1,0:T(8,128)(2,1)}, bf16[128,2048]{1,0:T(8,128)(2,1)}, u32[]{:S(2)}, u32[]{:S(2)}) collective-permute-start(bf16[128,2048]{1,0:T(8,128)(2,1)} %collective-permute-done.5), channel_id=1, source_target_pairs={{0,1},{1,2},{2,3},{3,4},{4,5},{5,6},{6,7},{7,0},{8,9},{9,10},{10,1... | collective-permute-start | bytes 1572872 | tf_op jit(solution)/shard_map/ppermute | solution.py:18
  118.8 2.2 multiply_reduce_fusion.1
  121.0 0.9 fusion.72
  122.7 4.1 %all-to-all-start = ((bf16[8,256,128]{1,2,0:T(8,128)(2,1)}), bf16[8,256,128]{1,2,0:T(8,128)(2,1)}, u32[]{:S(2)}, u32[]{:S(2)}) async-start(bf16[8,256,128]{1,2,0:T(8,128)(2,1)} %broadcast_in_dim.32), calls=%async_computation | async-start | bytes 1048576 | tf_op jit(solution)/shard_map/all_to_all | solution.py:70
  126.9 1.9 constant_dynamic-update-slice_fusion.15
  128.8 1.9 constant_dynamic-update-slice_fusion.14
  130.7 0.8 constant_dynamic-update-slice_fusion.13
  131.6 0.9 constant_dynamic-update-slice_fusion.12
  134.1 0.8 constant_dynamic-update-slice_fusion.9
  135.8 1.9 constant_dynamic-update-slice_fusion.7
  137.7 1.9 constant_dynamic-update-slice_fusion.6
  139.6 0.9 constant_dynamic-update-slice_fusion.5
  142.2 0.9 constant_dynamic-update-slice_fusion.2
  143.0 0.9 constant_dynamic-update-slice_fusion.1
  143.9 0.9 constant_dynamic-update-slice_fusion
  144.8 4.0 %multiply_reduce_fusion = (f32[256]{0:T(256)S(1)}, f32[256,2048]{1,0:T(8,128)S(1)}) fusion(bf16[256,1024]{0,1:T(8,128)(2,1)} %bitcast.42, bf16[2048,2048]{1,0:T(8,128)(2,1)} %constant_dynamic-update-slice_fusion, s32[]{:T(128)S(6)} %select_n.294, bf16[256,2048]{1,0:T(8,128)(2,1)} %param.14), kind=kOutput, calls=%fused_computation.47 | convolution fusion | flops 1075838720 | bytes 7865348 | tf_op jit(solution)/shard_map/dot_general | solution.py:198
  148.8 115.8 %all-gather.7.cloned.1.call-done = bf16[2048,2048]{1,0:T(8,128)(2,1)} async-done(((bf16[32,2048]{1,0:T(8,128)(2,1)}), bf16[2048,2048]{1,0:T(8,128)(2,1)}) %all-gather.7.cloned.1.call-update) | async-done | bytes 8388624 | tf_op jit(solution)/shard_map/all_gather | solution.py:82
  264.7 6.8 %fusion.37 = bf16[256,2048]{1,0:T(8,128)(2,1)} fusion(bf16[2048,2048]{1,0:T(8,128)(2,1)} %all-gather.7.cloned.1.call-done, f32[256,2048]{1,0:T(8,128)S(1)} %get-tuple-element.142, f32[2048]{0:T(1024)S(1)} %copy-done.9, f32[256]{0:T(256)S(1)} %add_rsqrt_fusion), kind=kOutput, calls=%fused_computation.44 | convolution fusion | flops 2150367232 | bytes 11543552 | tf_op jit(solution)/shard_map/dot_general | solution.py:210
  271.5 12.7 %all-to-all-start.1 = ((bf16[8,32,2048]{2,1,0:T(8,128)(2,1)}), bf16[8,32,2048]{2,1,0:T(8,128)(2,1)S(1)}, u32[]{:S(2)}, u32[]{:S(2)}) async-start(bf16[8,32,2048]{2,1,0:T(8,128)(2,1)} %bitcast.43), calls=%async_computation.1 | async-start | bytes 2097152 | tf_op jit(solution)/shard_map/all_to_all | solution.py:94
  284.2 15.0 %all-to-all-done.1 = bf16[8,32,2048]{2,1,0:T(8,128)(2,1)S(1)} async-done(((bf16[8,32,2048]{2,1,0:T(8,128)(2,1)}), bf16[8,32,2048]{2,1,0:T(8,128)(2,1)S(1)}, u32[]{:S(2)}, u32[]{:S(2)}) %all-to-all-start.1) | async-done | bytes 1048608 | tf_op jit(solution)/shard_map/all_to_all | solution.py:94
  299.3 1.0 add_convert_fusion
  300.4 18.3 %all_to_all.15 = bf16[8,32,2048]{2,1,0:T(8,128)(2,1)S(1)} all-to-all(bf16[8,32,2048]{2,1,0:T(8,128)(2,1)S(1)} %broadcast_in_dim.33), channel_id=1, replica_groups=mesh['sp_0'=16,'sp_1'=4,'tp'=8] {'tp'}, dimensions={0} | all-to-all | bytes 2097152 | tf_op jit(solution)/shard_map/all_to_all | solution.py:70
  318.7 1.0 copy.95
  (98 shorter events, 14.4 us)
Async XLA Ops:
  6.5 99.8 %all-gather.9.cloned.1.call-start = ((), (), s32[]{:S(2)}) async-start(), calls=%async_computation.4 | async-start | bytes 1183744 | tf_op jit(solution)/shard_map/all_gather | solution.py:38
  9.8 1.0 copy-start.1
  10.9 27.6 %copy-start.2 = (bf16[32,1024]{1,0:T(8,128)(2,1)S(1)}, bf16[32,1024]{1,0:T(8,128)(2,1)}, u32[]{:S(2)}) copy-start(bf16[32,1024]{1,0:T(8,128)(2,1)} %param.25) | copy-start | bytes 196612
  10.9 27.6 %copy-start.3 = (bf16[32,1024]{1,0:T(8,128)(2,1)S(1)}, bf16[32,1024]{1,0:T(8,128)(2,1)}, u32[]{:S(2)}) copy-start(bf16[32,1024]{1,0:T(8,128)(2,1)} %param.24) | copy-start | bytes 196612
  10.9 28.3 %copy-start = (bf16[128,2048]{1,0:T(8,128)(2,1)S(1)}, bf16[128,2048]{1,0:T(8,128)(2,1)}, u32[]{:S(2)}) copy-start(bf16[128,2048]{1,0:T(8,128)(2,1)} %param.22) | copy-start | bytes 1572868
  37.1 2.0 copy-start.6
  37.1 2.0 copy-start.7
  37.1 2.0 copy-start.8
  37.6 1.5 copy-start.5
  38.4 226.2 %all-gather.7.cloned.1.call-start = ((), (), s32[]{:S(2)}) async-start(), calls=%async_computation.3 | async-start | bytes 8519680 | tf_op jit(solution)/shard_map/all_gather | solution.py:82
  39.2 10.8 %collective-permute-start = (bf16[128,2048]{1,0:T(8,128)(2,1)S(1)}, bf16[128,2048]{1,0:T(8,128)(2,1)S(1)}, u32[]{:S(2)}, u32[]{:S(2)}) collective-permute-start(bf16[128,2048]{1,0:T(8,128)(2,1)S(1)} %copy-done), channel_id=1, source_target_pairs={{0,1},{1,2},{2,3},{3,4},{4,5},{5,6},{6,7},{7,0},{8,9},{9,10},{10,1... | collective-permute-start | bytes 1572872 | tf_op jit(solution)/shard_map/ppermute | solution.py:18
  50.0 8.8 %collective-permute-start.1 = (bf16[128,2048]{1,0:T(8,128)(2,1)S(1)}, bf16[128,2048]{1,0:T(8,128)(2,1)S(1)}, u32[]{:S(2)}, u32[]{:S(2)}) collective-permute-start(bf16[128,2048]{1,0:T(8,128)(2,1)S(1)} %collective-permute-done), channel_id=1, source_target_pairs={{0,1},{1,2},{2,3},{3,4},{4,5},{5,6},{6,7},{7,0},{8,9},{9,10},{10,1... | collective-permute-start | bytes 1572872 | tf_op jit(solution)/shard_map/ppermute | solution.py:18
  58.8 9.8 %collective-permute-start.2 = (bf16[128,2048]{1,0:T(8,128)(2,1)S(1)}, bf16[128,2048]{1,0:T(8,128)(2,1)S(1)}, u32[]{:S(2)}, u32[]{:S(2)}) collective-permute-start(bf16[128,2048]{1,0:T(8,128)(2,1)S(1)} %collective-permute-done.1), channel_id=1, source_target_pairs={{0,1},{1,2},{2,3},{3,4},{4,5},{5,6},{6,7},{7,0},{8,9},{9,10},{10,1... | collective-permute-start | bytes 1572872 | tf_op jit(solution)/shard_map/ppermute | solution.py:18
  68.6 9.8 %collective-permute-start.3 = (bf16[128,2048]{1,0:T(8,128)(2,1)S(1)}, bf16[128,2048]{1,0:T(8,128)(2,1)S(1)}, u32[]{:S(2)}, u32[]{:S(2)}) collective-permute-start(bf16[128,2048]{1,0:T(8,128)(2,1)S(1)} %collective-permute-done.2), channel_id=1, source_target_pairs={{0,1},{1,2},{2,3},{3,4},{4,5},{5,6},{6,7},{7,0},{8,9},{9,10},{10,1... | collective-permute-start | bytes 1572872 | tf_op jit(solution)/shard_map/ppermute | solution.py:18
  78.5 9.8 %collective-permute-start.4 = (bf16[128,2048]{1,0:T(8,128)(2,1)S(1)}, bf16[128,2048]{1,0:T(8,128)(2,1)S(1)}, u32[]{:S(2)}, u32[]{:S(2)}) collective-permute-start(bf16[128,2048]{1,0:T(8,128)(2,1)S(1)} %collective-permute-done.3), channel_id=1, source_target_pairs={{0,1},{1,2},{2,3},{3,4},{4,5},{5,6},{6,7},{7,0},{8,9},{9,10},{10,1... | collective-permute-start | bytes 1572872 | tf_op jit(solution)/shard_map/ppermute | solution.py:18
  88.3 18.9 %collective-permute-start.5 = (bf16[128,2048]{1,0:T(8,128)(2,1)S(1)}, bf16[128,2048]{1,0:T(8,128)(2,1)}, u32[]{:S(2)}, u32[]{:S(2)}) collective-permute-start(bf16[128,2048]{1,0:T(8,128)(2,1)S(1)} %collective-permute-done.4), channel_id=1, source_target_pairs={{0,1},{1,2},{2,3},{3,4},{4,5},{5,6},{6,7},{7,0},{8,9},{9,10},{10,1... | collective-permute-start | bytes 1572872 | tf_op jit(solution)/shard_map/ppermute | solution.py:18
  107.2 19.7 %collective-permute-start.6 = (bf16[128,2048]{1,0:T(8,128)(2,1)}, bf16[128,2048]{1,0:T(8,128)(2,1)}, u32[]{:S(2)}, u32[]{:S(2)}) collective-permute-start(bf16[128,2048]{1,0:T(8,128)(2,1)} %collective-permute-done.5), channel_id=1, source_target_pairs={{0,1},{1,2},{2,3},{3,4},{4,5},{5,6},{6,7},{7,0},{8,9},{9,10},{10,1... | collective-permute-start | bytes 1572872 | tf_op jit(solution)/shard_map/ppermute | solution.py:18
  122.7 22.0 %all-to-all-start = ((bf16[8,256,128]{1,2,0:T(8,128)(2,1)}), bf16[8,256,128]{1,2,0:T(8,128)(2,1)}, u32[]{:S(2)}, u32[]{:S(2)}) async-start(bf16[8,256,128]{1,2,0:T(8,128)(2,1)} %broadcast_in_dim.32), calls=%async_computation | async-start | bytes 1048576 | tf_op jit(solution)/shard_map/all_to_all | solution.py:70
  135.8 128.9 %copy-start.9 = (f32[2048]{0:T(1024)S(1)}, f32[2048]{0:T(1024)}, u32[]{:S(2)}) copy-start(f32[2048]{0:T(1024)} %param.23) | copy-start | bytes 24580
  148.8 122.7 %copy-start.4 = (f32[256,2048]{1,0:T(8,128)}, f32[256,2048]{1,0:T(8,128)S(1)}, u32[]{:S(2)}) copy-start(f32[256,2048]{1,0:T(8,128)S(1)} %get-tuple-element.142) | copy-start | bytes 6291460
  271.5 27.6 %all-to-all-start.1 = ((bf16[8,32,2048]{2,1,0:T(8,128)(2,1)}), bf16[8,32,2048]{2,1,0:T(8,128)(2,1)S(1)}, u32[]{:S(2)}, u32[]{:S(2)}) async-start(bf16[8,32,2048]{2,1,0:T(8,128)(2,1)} %bitcast.43), calls=%async_computation.1 | async-start | bytes 2097152 | tf_op jit(solution)/shard_map/all_to_all | solution.py:94
Sparse Core Ops, SparseCore 0:
  38.6 67.7 all-gather.8
  109.3 155.2 all-gather.6
